TPU v7x, 32 devices: a whole 2x2x4 slice. The times are simulated.
32 devices in a mesh: ep: 8 (over z, y), tp: 4 (over x, core).
Axes of the slice: x: 2, y: 2, z: 4, core: 2. Of those that a mesh axis runs over, the one named last changes fastest.
Arguments:
- tokens: bfloat16 [16, 2048], P('ep'), may hold values from -6 to 6
- state_c: float32 [16, 8, 128, 256], P('ep', 'tp'), may hold values from -0.8 to 0.8
- state_n: float32 [16, 8, 128], P('ep', 'tp'), may hold values from -0.8 to 0.8
- state_m: float32 [16, 8], P('ep', 'tp'), may hold values from -2 to 2
- mix_gain: float32 [2048], replicated, may hold values from 0.1 to 1.9
- w_query: bfloat16 [2048, 1024], P('ep', 'tp'), may hold values from -0.125 to 0.125
- w_key: bfloat16 [2048, 1024], P('ep', 'tp'), may hold values from -0.125 to 0.125
- w_value: bfloat16 [2048, 2048], P('ep', 'tp'), may hold values from -0.125 to 0.125
- w_input_gate: bfloat16 [2048, 8], replicated, may hold values from -0.125 to 0.125
- w_forget_gate: bfloat16 [2048, 8], replicated, may hold values from -0.125 to 0.125
- forget_bias: float32 [8], replicated, may hold values from -1 to 4
- w_output: bfloat16 [2048, 2048], P('tp', 'ep'), may hold values from -0.125 to 0.125
- moe_gain: float32 [2048], replicated, may hold values from 0.1 to 1.9
- w_group: bfloat16 [2048, 4], replicated, may hold values from -0.25 to 0.25
- expert_ids: int32 [16, 2], P('ep'), may hold values from 0 to 7, all different within a row; in each aligned block of 2 rows (0 to 1, 2 to 3, ...) at most 1 rows name the same one
- expert_weight: float32 [16, 2], P('ep'), may hold values from 0.1 to 1
- w_exp_gate: bfloat16 [8, 2048, 512], P('ep', None, 'tp'), may hold values from -0.125 to 0.125
- w_exp_up: bfloat16 [8, 2048, 512], P('ep', None, 'tp'), may hold values from -0.25 to 0.25
- w_exp_down: bfloat16 [8, 512, 2048], P('ep', 'tp'), may hold values from -1 to 1
- w_dense: bfloat16 [2048, 2048], P('ep', 'tp'), may hold values from -0.125 to 0.125
- w_dense_gate: bfloat16 [2048], replicated, may hold values from -0.125 to 0.125
Outputs:
- mixed: bfloat16 [16, 2048], P('ep', 'tp')
- new_c: float32 [16, 8, 128, 256], P('ep', 'tp')
- new_n: float32 [16, 8, 128], P('ep', 'tp')
- new_m: float32 [16, 8], P('ep', 'tp')
Inputs may be any that keep to these rules, and one draw needn't show every extreme that they name: `expert_ids`: each row names 2 different experts. In each aligned block of 2 rows (the rows of one index of ep) no expert is named by more than 1 row, a bound that some block reaches. Every expert is named by some row.
All inputs are finite; a program needn't handle non-finite values.
Results may differ from a plain program's by a relative error of at most 0.025.
Values may be sent and summed in bfloat16 or wider, within the bound.
A program may use at most 64 MiB of HBM per device.

v0:
```python
import jax
import jax.numpy as jnp
from jax import lax
from jax.sharding import PartitionSpec as P

CAP = 1


eps = 1e-06


def rms_norm(values, gain):
    widened = values.astype(jnp.float32)
    inverse = lax.rsqrt(jnp.mean(widened * widened, axis=-1, keepdims=True) + eps)
    return (widened * inverse * gain).astype(jnp.bfloat16)


def rounded(values):
    return lax.optimization_barrier(values.astype(jnp.bfloat16)).astype(jnp.float32)


def memory_step(query_rows, key_rows, value_rows, in_gate, forget, state_c, state_n, state_m):
    seq_count, head_count = state_m.shape
    q_heads = query_rows.reshape(seq_count, head_count, -1)
    k_heads = key_rows.reshape(seq_count, head_count, -1) * q_heads.shape[-1] ** (-0.5)
    v_heads = value_rows.reshape(seq_count, head_count, -1)
    new_m = jnp.maximum(forget + state_m, in_gate)
    decay = jnp.exp(forget + state_m - new_m)
    inflow = jnp.exp(in_gate - new_m)
    new_c = (
        decay[..., None, None] * state_c
        + (inflow[..., None] * k_heads)[..., :, None] * v_heads[..., None, :]
    )
    new_n = decay[..., None] * state_n + inflow[..., None] * k_heads
    numer = jnp.einsum("shd,shde->she", q_heads, new_c, precision=lax.Precision.HIGHEST)
    denom = jnp.maximum(jnp.abs(jnp.sum(q_heads * new_n, axis=-1)), 1.0)
    heads = (numer / denom[..., None]).astype(jnp.bfloat16).reshape(seq_count, -1)
    return (heads, new_c, new_n, new_m)


def per_device(
    tokens,
    state_c,
    state_n,
    state_m,
    mix_gain,
    w_query,
    w_key,
    w_value,
    w_input_gate,
    w_forget_gate,
    forget_bias,
    w_output,
    moe_gain,
    w_group,
    expert_ids,
    expert_weight,
    w_exp_gate,
    w_exp_up,
    w_exp_down,
    w_dense,
    w_dense_gate,
):
    seq_count = tokens.shape[0]
    width = tokens.shape[1]
    tp_count = lax.axis_size("tp")
    ep_count = lax.axis_size("ep")
    tp_rank = lax.axis_index("tp")
    head_count = state_m.shape[1]
    qk_cols = w_query.shape[1]
    share = width // tp_count
    normed = rms_norm(tokens, mix_gain)
    spread_cols = lax.all_to_all(normed, "ep", split_axis=1, concat_axis=0, tiled=True)
    joined = jnp.concatenate([w_query, w_key, w_value], axis=1)
    token_rows = spread_cols
    summed = lax.psum_scatter(
        jnp.dot(token_rows, joined, preferred_element_type=jnp.float32),
        "ep",
        scatter_dimension=0,
        tiled=True,
    )
    query_sum = summed[:, :qk_cols]
    key_sum = summed[:, qk_cols : 2 * qk_cols]
    value_sum = summed[:, 2 * qk_cols :]
    query_rows = rounded(query_sum)
    key_rows = rounded(key_sum)
    value_rows = rounded(value_sum)
    gate_all = jnp.dot(normed, w_input_gate, preferred_element_type=jnp.float32)
    forget_all = jax.nn.log_sigmoid(
        jnp.dot(normed, w_forget_gate, preferred_element_type=jnp.float32) + forget_bias
    )
    in_gate = lax.dynamic_slice_in_dim(gate_all, tp_rank * head_count, head_count, 1)
    forget = lax.dynamic_slice_in_dim(forget_all, tp_rank * head_count, head_count, 1)
    heads, new_c, new_n, new_m = memory_step(
        query_rows, key_rows, value_rows, in_gate, forget, state_c, state_n, state_m
    )
    row_parts = jnp.dot(
        lax.all_gather(heads, "ep", axis=0, tiled=True),
        w_output,
        preferred_element_type=jnp.float32,
    ).astype(jnp.bfloat16)
    partial_value = lax.all_to_all(row_parts, "ep", split_axis=0, concat_axis=1, tiled=True).astype(
        jnp.float32
    )
    mixer_sum = lax.psum(partial_value.astype(jnp.bfloat16), "tp").astype(jnp.float32)
    residual = (tokens.astype(jnp.float32) + mixer_sum).astype(jnp.bfloat16)
    normed2 = rms_norm(residual, moe_gain)
    group_count = w_group.shape[1]
    group_prob = jax.nn.softmax(
        jnp.dot(normed2, w_group, preferred_element_type=jnp.float32), axis=-1
    )
    experts_here = w_exp_gate.shape[0]
    expert_count = experts_here * ep_count
    per_group = expert_count // group_count
    top_count = expert_ids.shape[1]
    member = (expert_ids // per_group)[..., None] == jnp.arange(group_count, dtype=jnp.int32)[
        None, None, :
    ]
    picked = jnp.sum(jnp.where(member, group_prob[:, None, :], 0.0), axis=-1)
    route = picked * expert_weight / jnp.sum(expert_weight, axis=1, keepdims=True)
    flat_ids = expert_ids.reshape(-1)
    assigned = flat_ids[:, None] == jnp.arange(expert_count, dtype=jnp.int32)[None, :]
    ranks = jnp.cumsum(assigned.astype(jnp.int32), axis=0) - 1
    own_rank = jnp.sum(jnp.where(assigned, ranks, 0), axis=1)
    slot_index = flat_ids * CAP + own_rank
    placing = (
        jnp.arange(expert_count * CAP, dtype=jnp.int32)[:, None] == slot_index[None, :]
    ).astype(jnp.bfloat16)
    repeated = jnp.repeat(normed2, top_count, axis=0)
    outgoing = jnp.dot(placing, repeated, preferred_element_type=jnp.float32).astype(jnp.bfloat16)
    outgoing = outgoing.reshape(expert_count, CAP, width)
    arrived = lax.all_to_all(outgoing, "ep", split_axis=0, concat_axis=0, tiled=True)
    slots = arrived.shape[1]
    grid_rows = arrived.reshape(ep_count, experts_here, slots, width)
    gate_act = jnp.einsum(
        "sxnd,xdf->sxnf", grid_rows, w_exp_gate, preferred_element_type=jnp.float32
    )
    up_act = jnp.einsum("sxnd,xdf->sxnf", grid_rows, w_exp_up, preferred_element_type=jnp.float32)
    hidden = (jax.nn.silu(gate_act) * up_act).astype(jnp.bfloat16)
    down_part = jnp.einsum("sxnf,xfd->sxnd", hidden, w_exp_down, preferred_element_type=jnp.float32)
    reduced = lax.psum_scatter(
        down_part.astype(jnp.bfloat16), "tp", scatter_dimension=3, tiled=True
    )
    returned = lax.all_to_all(
        reduced.reshape(expert_count, slots, share), "ep", split_axis=0, concat_axis=0, tiled=True
    )
    picked_rows = jnp.einsum(
        "ca,cd->ad",
        placing,
        returned.reshape(expert_count * CAP, share),
        preferred_element_type=jnp.float32,
    )
    moe = jnp.sum(route[..., None] * picked_rows.reshape(seq_count, top_count, share), axis=1)
    dense_cols = lax.all_to_all(normed2, "ep", split_axis=1, concat_axis=0, tiled=True)
    token_rows = dense_cols
    dense_raw = lax.psum_scatter(
        jnp.dot(token_rows, w_dense, preferred_element_type=jnp.float32),
        "ep",
        scatter_dimension=0,
        tiled=True,
    )
    dense_gate = jax.nn.sigmoid(jnp.dot(normed2, w_dense_gate, preferred_element_type=jnp.float32))
    own_cols = lax.dynamic_slice_in_dim(residual, tp_rank * share, share, 1).astype(jnp.float32)
    mixed = (own_cols + moe + dense_gate[:, None] * dense_raw).astype(jnp.bfloat16)
    return (mixed, new_c, new_n, new_m)


def solution(mesh):
    placed = (
        P("ep", None),
        P("ep", "tp", None, None),
        P("ep", "tp", None),
        P("ep", "tp"),
        P(),
        P("ep", "tp"),
        P("ep", "tp"),
        P("ep", "tp"),
        P(),
        P(),
        P(),
        P("tp", "ep"),
        P(),
        P(),
        P("ep", None),
        P("ep", None),
        P("ep", None, "tp"),
        P("ep", None, "tp"),
        P("ep", "tp", None),
        P("ep", "tp"),
        P(),
    )
    return jax.shard_map(
        per_device,
        mesh=mesh,
        in_specs=placed,
        out_specs=(P("ep", "tp"), P("ep", "tp", None, None), P("ep", "tp", None), P("ep", "tp")),
        check_vma=False,
    )
```

profile of v0, /device:TPU:0, one launch (start us, length us, event | category | flops | bytes accessed | tf_op | source)
XLA Modules:
  0.0 200.7 jit_solution(5687725438537635701)
XLA Ops:
  7.2 0.9 fusion.27
  8.1 1.4 fusion.29
  9.5 7.4 %all-to-all-start = ((bf16[2,8,256]{2,0,1:T(2,128)(2,1)}), bf16[2,8,256]{2,0,1:T(2,128)(2,1)S(1)}, u32[]{:S(2)}, u32[]{:S(2)}) async-start(bf16[2,8,256]{2,0,1:T(2,128)(2,1)} %bitcast), calls=%async_computation | async-start | bytes 16384 | tf_op jit(solution)/shard_map/all_to_all | solution.py:73
  16.9 0.7 copy-done.14
  17.7 0.8 fusion.58
  18.5 0.9 fusion.48
  20.4 0.6 copy-done.20
  22.3 1.1 all-to-all-done
  23.5 1.2 fusion.11
  24.7 36.9 %all-reduce = bf16[16,1024]{1,0:T(8,128)(2,1)S(1)} all-reduce(f32[16,1024]{1,0:T(8,128)S(1)} %fusion.11), channel_id=2, replica_groups=mesh['ep'=8,'tp'=4] {'ep'}, use_global_device_ids=true, to_apply=%region_1.0.clone | all-reduce | flops 16384 | bytes 98304
  62.3 0.7 slice-done
  62.9 0.7 multiply_reduce_fusion
  64.2 26.2 %all-gather = bf16[8,2,512]{2,1,0:T(2,128)(2,1)S(1)} all-gather(bf16[1,2,512]{2,1,0:T(2,128)(2,1)S(1)} %reshape.161), channel_id=1, replica_groups=mesh['ep'=8,'tp'=4] {'ep'}, dimensions={0}, use_global_device_ids=true | all-gather | bytes 18432 | tf_op jit(solution)/shard_map/all_gather | solution.py:98
  91.3 3.3 %all-to-all-start.1 = ((bf16[8,2,256]{2,1,0:T(2,128)(2,1)}), bf16[8,2,256]{2,1,0:T(2,128)(2,1)S(1)}, u32[]{:S(2)}, u32[]{:S(2)}) async-start(bf16[8,2,256]{2,1,0:T(2,128)(2,1)} %all_to_all.52), calls=%async_computation.1 | async-start | bytes 16384 | tf_op jit(solution)/shard_map/all_to_all | solution.py:102
  94.8 6.2 %all-to-all-done.1 = bf16[8,2,256]{2,1,0:T(2,128)(2,1)S(1)} async-done(((bf16[8,2,256]{2,1,0:T(2,128)(2,1)}), bf16[8,2,256]{2,1,0:T(2,128)(2,1)S(1)}, u32[]{:S(2)}, u32[]{:S(2)}) %all-to-all-start.1) | async-done | bytes 8224 | tf_op jit(solution)/shard_map/all_to_all | solution.py:102
  101.1 5.7 %psum.7 = bf16[2,2048]{1,0:T(2,128)(2,1)S(1)} all-reduce(bf16[2,2048]{1,0:T(2,128)(2,1)S(1)} %bitcast.93), channel_id=1, replica_groups=mesh['ep'=8,'tp'=4] {'tp'}, use_global_device_ids=true, to_apply=%region_3.4 | all-reduce | flops 4096 | bytes 16384 | tf_op jit(solution)/shard_map/psum | solution.py:105
  107.0 0.7 fusion.26
  107.6 0.9 fusion.57
  108.8 0.7 broadcast_in_dim.16
  109.6 3.4 %all-to-all-start.4 = ((bf16[2,8,256]{2,0,1:T(2,128)(2,1)}), bf16[2,8,256]{2,0,1:T(2,128)(2,1)S(1)}, u32[]{:S(2)}, u32[]{:S(2)}) async-start(bf16[2,8,256]{2,0,1:T(2,128)(2,1)} %bitcast.23), calls=%async_computation.5 | async-start | bytes 16384 | tf_op jit(solution)/shard_map/all_to_all | solution.py:154
  113.0 0.9 fusion.10
  114.7 0.7 reduce
  115.4 0.6 reshape.175
  116.0 3.5 %all-to-all-done.4 = bf16[2,8,256]{2,0,1:T(2,128)(2,1)S(1)} async-done(((bf16[2,8,256]{2,0,1:T(2,128)(2,1)}), bf16[2,8,256]{2,0,1:T(2,128)(2,1)S(1)}, u32[]{:S(2)}, u32[]{:S(2)}) %all-to-all-start.4) | async-done | bytes 8224 | tf_op jit(solution)/shard_map/all_to_all | solution.py:154
  119.5 3.3 %all-to-all-start.2 = ((bf16[8,2,1024]{2,1,0:T(2,128)(2,1)}), bf16[8,2,1024]{2,1,0:T(2,128)(2,1)S(1)}, u32[]{:S(2)}, u32[]{:S(2)}) async-start(bf16[8,2,1024]{2,1,0:T(2,128)(2,1)} %reshape.175), calls=%async_computation.2 | async-start | bytes 65536 | tf_op jit(solution)/shard_map/all_to_all | solution.py:132
  123.0 6.5 %all-to-all-done.2 = bf16[8,2,1024]{2,1,0:T(2,128)(2,1)S(1)} async-done(((bf16[8,2,1024]{2,1,0:T(2,128)(2,1)}), bf16[8,2,1024]{2,1,0:T(2,128)(2,1)S(1)}, u32[]{:S(2)}, u32[]{:S(2)}) %all-to-all-start.2) | async-done | bytes 32800 | tf_op jit(solution)/shard_map/all_to_all | solution.py:132
  129.7 1.0 fusion.1
  130.8 17.1 %reduce-scatter.2.cloned.1.call-done = bf16[8,1,1,512]{3,0,2,1:T(8,128)(2,1)} async-done(((bf16[8,1,1,2048]{3,0,2,1:T(8,128)(2,1)}), bf16[8,1,1,512]{3,0,2,1:T(8,128)(2,1)}) %reduce-scatter.2.cloned.1.call-update) | async-done | bytes 8208 | tf_op jit(solution)/shard_map/reduce_scatter | solution.py:141
  148.0 1.3 reduce.1
  149.9 5.5 %all-to-all-start.3 = ((bf16[8,2,256]{2,1,0:T(2,128)(2,1)}), bf16[8,2,256]{2,1,0:T(2,128)(2,1)S(1)}, u32[]{:S(2)}, u32[]{:S(2)}) async-start(bf16[8,2,256]{2,1,0:T(2,128)(2,1)} %reshape.177), calls=%async_computation.4 | async-start | bytes 16384 | tf_op jit(solution)/shard_map/all_to_all | solution.py:144
  155.4 37.6 %all-reduce.1 = f32[16,512]{1,0:T(8,128)S(1)} all-reduce(f32[16,512]{1,0:T(8,128)S(1)} %fusion.60), channel_id=4, replica_groups=mesh['ep'=8,'tp'=4] {'ep'}, use_global_device_ids=true, to_apply=%region_13.14.clone | all-reduce | flops 8192 | bytes 65536
  193.1 0.7 fusion.37
  (89 shorter events, 6.4 us)
Async XLA Ops:
  7.2 122.5 %copy-start = (bf16[1,128,2048]{2,1,0:T(8,128)(2,1)S(1)}, bf16[1,128,2048]{2,1,0:T(8,128)(2,1)}, u32[]{:S(2)}) copy-start(bf16[1,128,2048]{2,1,0:T(8,128)(2,1)} %param.39) | copy-start | bytes 1572868
  7.2 0.9 copy-start.7
  7.2 10.5 %copy-start.17 = (bf16[2048,8]{0,1:T(8,128)(2,1)S(1)}, bf16[2048,8]{0,1:T(8,128)(2,1)}, u32[]{:S(2)}) copy-start(bf16[2048,8]{0,1:T(8,128)(2,1)} %param.29) | copy-start | bytes 98308
  9.5 9.0 %copy-start.19 = (f32[8]{0:T(128)S(1)}, f32[8]{0:T(128)}, u32[]{:S(2)}) copy-start(f32[8]{0:T(128)} %param.31) | copy-start | bytes 100
  9.5 14.0 %all-to-all-start = ((bf16[2,8,256]{2,0,1:T(2,128)(2,1)}), bf16[2,8,256]{2,0,1:T(2,128)(2,1)S(1)}, u32[]{:S(2)}, u32[]{:S(2)}) async-start(bf16[2,8,256]{2,0,1:T(2,128)(2,1)} %bitcast), calls=%async_computation | async-start | bytes 16384 | tf_op jit(solution)/shard_map/all_to_all | solution.py:73
  16.9 0.7 copy-start.14
  16.9 6.5 %copy-start.16 = (bf16[256,256]{1,0:T(8,128)(2,1)S(1)}, bf16[256,256]{1,0:T(8,128)(2,1)}, u32[]{:S(2)}) copy-start(bf16[256,256]{1,0:T(8,128)(2,1)} %param.27) | copy-start | bytes 393220
  18.5 0.9 copy-start.15
  19.5 0.6 copy-start.12
  20.4 0.7 copy-start.20
  23.5 40.1 %copy-start.2 = (f32[2,2,128,256]{3,2,1,0:T(8,128)S(1)}, f32[2,2,128,256]{3,2,1,0:T(8,128)}, u32[]{:S(2)}) copy-start(f32[2,2,128,256]{3,2,1,0:T(8,128)} %param.22) | copy-start | bytes 1572868
  61.6 0.6 copy-start.8
  62.2 0.7 copy-start.13
  62.2 0.7 slice-start
  63.8 44.8 %copy-start.1 = (f32[2,2,128,256]{3,2,1,0:T(8,128)}, f32[2,2,128,256]{3,2,1,0:T(8,128)S(1)}, u32[]{:S(2)}) copy-start(f32[2,2,128,256]{3,2,1,0:T(8,128)S(1)} %multiply_add_fusion) | copy-start | bytes 1572868
  63.8 26.7 %copy-start.6 = (bf16[512,256]{1,0:T(8,128)(2,1)S(1)}, bf16[512,256]{1,0:T(8,128)(2,1)}, u32[]{:S(2)}) copy-start(bf16[512,256]{1,0:T(8,128)(2,1)} %param.32) | copy-start | bytes 786436
  63.8 30.9 %copy-start.10 = (bf16[2048]{0:T(1024)(128)(2,1)S(1)}, bf16[2048]{0:T(1024)(128)(2,1)}, u32[]{:S(2)}) copy-start(bf16[2048]{0:T(1024)(128)(2,1)} %param.41) | copy-start | bytes 12292
  63.8 30.9 %copy-start.11 = (f32[2,2]{1,0:T(2,128)S(1)}, f32[2,2]{1,0:T(2,128)}, u32[]{:S(2)}) copy-start(f32[2,2]{1,0:T(2,128)} %param.36) | copy-start | bytes 52
  63.8 43.1 %copy-start.9 = (f32[2048]{0:T(1024)S(1)}, f32[2048]{0:T(1024)}, u32[]{:S(2)}) copy-start(f32[2048]{0:T(1024)} %param.33) | copy-start | bytes 24580
  63.8 43.8 %copy-start.18 = (bf16[2048,4]{0,1:T(4,128)(2,1)S(1)}, bf16[2048,4]{0,1:T(4,128)(2,1)}, u32[]{:S(2)}) copy-start(bf16[2048,4]{0,1:T(4,128)(2,1)} %param.34) | copy-start | bytes 49156
  64.2 65.3 %copy-start.3 = (bf16[1,2048,128]{2,1,0:T(8,128)(2,1)S(1)}, bf16[1,2048,128]{2,1,0:T(8,128)(2,1)}, u32[]{:S(2)}) copy-start(bf16[1,2048,128]{2,1,0:T(8,128)(2,1)} %param.37) | copy-start | bytes 1572868
  91.3 9.8 %all-to-all-start.1 = ((bf16[8,2,256]{2,1,0:T(2,128)(2,1)}), bf16[8,2,256]{2,1,0:T(2,128)(2,1)S(1)}, u32[]{:S(2)}, u32[]{:S(2)}) async-start(bf16[8,2,256]{2,1,0:T(2,128)(2,1)} %all_to_all.52), calls=%async_computation.1 | async-start | bytes 16384 | tf_op jit(solution)/shard_map/all_to_all | solution.py:102
  109.6 20.1 %copy-start.4 = (bf16[1,2048,128]{2,1,0:T(8,128)(2,1)S(1)}, bf16[1,2048,128]{2,1,0:T(8,128)(2,1)}, u32[]{:S(2)}) copy-start(bf16[1,2048,128]{2,1,0:T(8,128)(2,1)} %param.38) | copy-start | bytes 1572868
  109.6 9.9 %all-to-all-start.4 = ((bf16[2,8,256]{2,0,1:T(2,128)(2,1)}), bf16[2,8,256]{2,0,1:T(2,128)(2,1)S(1)}, u32[]{:S(2)}, u32[]{:S(2)}) async-start(bf16[2,8,256]{2,0,1:T(2,128)(2,1)} %bitcast.23), calls=%async_computation.5 | async-start | bytes 16384 | tf_op jit(solution)/shard_map/all_to_all | solution.py:154
  119.5 10.0 %all-to-all-start.2 = ((bf16[8,2,1024]{2,1,0:T(2,128)(2,1)}), bf16[8,2,1024]{2,1,0:T(2,128)(2,1)S(1)}, u32[]{:S(2)}, u32[]{:S(2)}) async-start(bf16[8,2,1024]{2,1,0:T(2,128)(2,1)} %reshape.175), calls=%async_computation.2 | async-start | bytes 65536 | tf_op jit(solution)/shard_map/all_to_all | solution.py:132
  122.8 25.1 %reduce-scatter.2.cloned.1.call-start = ((), (), s32[]{:S(2)}) async-start(), calls=%async_computation.6 | async-start | bytes 40960 | tf_op jit(solution)/shard_map/reduce_scatter | solution.py:141
  129.7 1.0 copy-start.5
  149.9 43.1 %all-to-all-start.3 = ((bf16[8,2,256]{2,1,0:T(2,128)(2,1)}), bf16[8,2,256]{2,1,0:T(2,128)(2,1)S(1)}, u32[]{:S(2)}, u32[]{:S(2)}) async-start(bf16[8,2,256]{2,1,0:T(2,128)(2,1)} %reshape.177), calls=%async_computation.4 | async-start | bytes 16384 | tf_op jit(solution)/shard_map/all_to_all | solution.py:144
Sparse Core Ops, SparseCore 0:
  130.8 17.1 reduce-scatter.1
where the time goes:
time: 202 us; the launch traced here: 201 us
  blocking collectives  106 us (52%)
  waiting for transfers between devices  34.5 us (17%)
  starting transfers between devices  23.1 us (11%)
  between operations  15 us (7%)
  other arithmetic  7.76 us (4%)
  local copies, waits for them, and re-layouts  7.08 us (4%)
  matrix products  6.76 us (3%)
    unnamed x2, blocking collectives  74.5 us
    all_gather x1, blocking collectives, per_device(): lax.all_gather(heads, 'ep', axis=0, tiled=True)  26.2 us
    reduce_scatter x1, waiting for transfers between devices, per_device(): lax.psum_scatter(down_part.astype(jnp.bfloat16), 'tp', scatter_dimension=...  17.1 us
    all_to_all x1, starting transfers between devices, per_device(): lax.all_to_all(normed, 'ep', split_axis=1, concat_axis=0, tiled=True)  7.44 us
    all_to_all x1, waiting for transfers between devices, per_device(): lax.all_to_all(outgoing, 'ep', split_axis=0, concat_axis=0, tiled=True)  6.49 us
    all_to_all x1, waiting for transfers between devices, per_device(): lax.all_to_all(row_parts, 'ep', split_axis=0, concat_axis=1, tiled=True)  6.22 us
    psum x1, blocking collectives, per_device(): lax.psum(partial_value.astype(jnp.bfloat16), 'tp').astype(jnp.float32)  5.74 us
    all_to_all x1, starting transfers between devices, per_device(): lax.all_to_all(reduced.reshape(expert_count, slots, share), 'ep', split_a...  5.51 us
  transfers between devices with their start and end apart: 6, of which 5 were waited for; matrix products, arithmetic and copies ran while one was open for 3% of the time, Pallas kernels for 0%

commit v1 on v0

--- a/solution.py
+++ b/solution.py
@@ -1,6 +1,10 @@
+import functools
+
 import jax
 import jax.numpy as jnp
 from jax import lax
+from jax.experimental import pallas as pl
+from jax.experimental.pallas import tpu as pltpu
 from jax.sharding import PartitionSpec as P
 
 CAP = 1
@@ -165,7 +169,482 @@
     return (mixed, new_c, new_n, new_m)
 
 
+F32 = jnp.float32
+BF16 = jnp.bfloat16
+MESH = pl.DeviceIdType.MESH
+
+
+def fits(ep, tp, args):
+    tokens, state_c, w_query, w_exp_gate = args[0], args[1], args[5], args[16]
+    seqs, width = tokens.shape
+    dqk, dv = state_c.shape[2:]
+    return (
+        width % (ep * 128) == 0
+        and ep % tp == 0
+        and w_query.shape[1] % 128 == 0
+        and dqk % 128 == 0
+        and dv % 128 == 0
+        and (width // tp) % 128 == 0
+        and w_exp_gate.shape[0] == 1
+        and w_exp_gate.shape[2] % 128 == 0
+        and seqs == 2
+    )
+
+
+def step_kernel(
+    ep,
+    tp,
+    tokens,
+    state_c,
+    state_n,
+    state_m,
+    mix_gain,
+    w_query,
+    w_key,
+    w_value,
+    w_in_t,
+    w_forget_t,
+    forget_bias,
+    w_output,
+    moe_gain,
+    w_group_t,
+    ids,
+    weight,
+    w_gate,
+    w_up,
+    w_down,
+    w_dense,
+    w_dense_gate,
+    mixed,
+    out_c,
+    out_n,
+    out_m,
+    v_c,
+    v_qkv,
+    v_out,
+    v_gu,
+    v_down,
+    v_dense,
+    new_c,
+    send_a,
+    recv_a,
+    send_b,
+    recv_b,
+    send_c,
+    recv_c,
+    send_d,
+    recv_d,
+    blocks,
+    send_g,
+    recv_g,
+    send_f,
+    recv_f,
+    rows_scr,
+    small_scr,
+    local_sem,
+    ep_send,
+    ep_recv,
+    tp_send,
+    tp_recv,
+    f_send,
+    f_recv,
+):
+    me = lax.axis_index("ep")
+    mt = lax.axis_index("tp")
+    seqs, width = tokens.shape
+    heads = state_c.shape[1]
+    dqk, dv = state_c.shape[2:]
+    qk = heads * dqk
+    col = width // ep
+    share = width // tp
+    ff = w_gate.shape[2]
+    every = ep * seqs
+
+    copies = {}
+    plan = [
+        ("q", w_query, v_qkv.at[:, 0:qk]),
+        ("k", w_key, v_qkv.at[:, qk : 2 * qk]),
+        ("v", w_value, v_qkv.at[:, 2 * qk :]),
+        ("c", state_c, v_c),
+        ("o", w_output, v_out),
+        ("d", w_dense, v_dense),
+        ("g", w_gate.at[0], v_gu.at[:, 0:ff]),
+        ("u", w_up.at[0], v_gu.at[:, ff:]),
+        ("w", w_down.at[0], v_down),
+    ]
+    for number, (name, src, dst) in enumerate(plan):
+        copies[name] = pltpu.make_async_copy(src, dst, local_sem.at[number])
+        copies[name].start()
+
+    barrier = pltpu.get_barrier_semaphore()
+    for k in range(ep):
+        for j in range(tp):
+            if k or j:
+                pl.semaphore_signal(
+                    barrier,
+                    inc=1,
+                    device_id={"ep": lax.rem(me + k, ep), "tp": lax.rem(mt + j, tp)},
+                    device_id_type=MESH,
+                )
+
+    def to_ep(phase, k, src, dst):
+        return pltpu.make_async_remote_copy(
+            src_ref=src,
+            dst_ref=dst,
+            send_sem=ep_send.at[phase, k],
+            recv_sem=ep_recv.at[phase, k],
+            device_id={"ep": lax.rem(me + k, ep), "tp": mt},
+            device_id_type=MESH,
+        )
+
+    def source(k):
+        return lax.rem(me + (ep - k), ep)
+
+    sends = []
+    tok = tokens[...].astype(F32)
+    inverse = lax.rsqrt(jnp.mean(tok * tok, axis=-1, keepdims=True) + eps)
+    normed_f = tok * inverse * mix_gain[...]
+    normed = normed_f.astype(BF16)
+    both = jnp.concatenate([normed.astype(F32), tok], axis=0).astype(BF16)
+    for e in range(ep):
+        send_a[e] = both[:, e * col : (e + 1) * col]
+    recv_a[me] = send_a[me]
+
+    pl.semaphore_wait(barrier, ep * tp - 1)
+
+    order = sorted(range(1, ep), key=lambda k: -min(k, ep - k))
+    near = order[::-1]
+    for k in order:
+        copy = to_ep(0, k, send_a.at[lax.rem(me + k, ep)], recv_a.at[me])
+        copy.start()
+        sends.append(copy)
+
+    last = (((1,), (1,)), ((), ()))
+    gate_all = lax.dot_general(normed, w_in_t[...], last, preferred_element_type=F32)
+    pre = lax.dot_general(normed, w_forget_t[...], last, preferred_element_type=F32)
+    pre = pre + forget_bias[...]
+    forget_all = jnp.minimum(pre, 0.0) - jnp.log1p(jnp.exp(-jnp.abs(pre)))
+    lane = lax.broadcasted_iota(jnp.int32, gate_all.shape, 1)
+    decays, inflows, new_ms = [], [], []
+    for h in range(heads):
+        here = lane == mt * heads + h
+        in_gate = jnp.sum(jnp.where(here, gate_all, 0.0), axis=1, keepdims=True)
+        forget = jnp.sum(jnp.where(here, forget_all, 0.0), axis=1, keepdims=True)
+        kept = forget + state_m[:, h : h + 1]
+        top = jnp.maximum(kept, in_gate)
+        new_ms.append(top)
+        decays.append(jnp.exp(kept - top))
+        inflows.append(jnp.exp(in_gate - top))
+    for h in range(heads):
+        out_m[:, h : h + 1] = new_ms[h]
+
+    def piece(total, e):
+        return total[e * seqs : (e + 1) * seqs]
+
+    for name in ("q", "k", "v"):
+        copies[name].wait()
+    for k in near:
+        to_ep(0, k, send_a.at[0], recv_a.at[source(k)]).wait_recv()
+    arrived = [recv_a[e].astype(F32) for e in range(ep)]
+    rows = jnp.concatenate([a[:seqs] for a in arrived], axis=0).astype(BF16)
+    own_cols = jnp.concatenate([a[seqs:] for a in arrived], axis=0)
+    part = jnp.dot(rows, v_qkv[...], preferred_element_type=F32)
+    for e in range(ep):
+        send_b[e] = piece(part, e).astype(BF16)
+    recv_b[me] = send_b[me]
+    for k in order:
+        copy = to_ep(1, k, send_b.at[lax.rem(me + k, ep)], recv_b.at[me])
+        copy.start()
+        sends.append(copy)
+
+    copies["c"].wait()
+    for k in near:
+        to_ep(1, k, send_b.at[0], recv_b.at[source(k)]).wait_recv()
+    summed = recv_b[0].astype(F32)
+    for e in range(1, ep):
+        summed = summed + recv_b[e].astype(F32)
+    summed = summed.astype(BF16).astype(F32)
+    q_rows, k_rows, v_rows = [], [], []
+    for s in range(seqs):
+        for h in range(heads):
+            row = summed[s : s + 1]
+            q_rows.append(row[:, h * dqk : (h + 1) * dqk])
+            k_rows.append(
+                row[:, qk + h * dqk : qk + (h + 1) * dqk]
+                * (dqk ** (-0.5) * inflows[h][s : s + 1])
+            )
+            v_rows.append(row[:, 2 * qk + h * dv : 2 * qk + (h + 1) * dv])
+    upright = jnp.concatenate(q_rows + k_rows, axis=0).T
+    count = seqs * heads
+    head_rows = []
+    for s in range(seqs):
+        parts = []
+        for h in range(heads):
+            at = s * heads + h
+            decay = decays[h][s : s + 1]
+            q_col = upright[:, at : at + 1]
+            k_col = upright[:, count + at : count + at + 1]
+            fresh = decay * v_c[s, h] + k_col * v_rows[at]
+            new_c[s, h] = fresh
+            numer = jnp.sum(q_col * fresh, axis=0, keepdims=True)
+            fresh_n = decay * state_n[s, h : h + 1] + k_rows[at]
+            out_n[s, h : h + 1] = fresh_n
+            denom = jnp.sum(q_rows[at] * fresh_n, axis=1, keepdims=True)
+            parts.append(numer / jnp.maximum(jnp.abs(denom), 1.0))
+        head_rows.append(jnp.concatenate(parts, axis=1))
+    head_out = jnp.concatenate(head_rows, axis=0).astype(BF16)
+    send_c[...] = head_out
+    recv_c[me] = head_out
+    for k in order:
+        copy = to_ep(2, k, send_c, recv_c.at[me])
+        copy.start()
+        sends.append(copy)
+    write_c = pltpu.make_async_copy(new_c, out_c, local_sem.at[len(plan)])
+    write_c.start()
+
+    small = jnp.concatenate(
+        [
+            w_group_t[...].astype(F32),
+            w_dense_gate[...].astype(F32),
+            jnp.zeros((8 - w_group_t.shape[0] - 1, width), F32),
+        ],
+        axis=0,
+    ).astype(BF16)
+    small_scr[...] = small
+
+    copies["o"].wait()
+    for k in near:
+        to_ep(2, k, send_c, recv_c.at[source(k)]).wait_recv()
+    all_heads = jnp.concatenate([recv_c[e].astype(F32) for e in range(ep)], axis=0).astype(BF16)
+    out_part = jnp.dot(all_heads, v_out[...], preferred_element_type=F32).astype(BF16)
+    send_d[...] = out_part
+    recv_d[mt] = out_part
+
+    def to_tp(j, dst):
+        return pltpu.make_async_remote_copy(
+            src_ref=send_d,
+            dst_ref=dst,
+            send_sem=tp_send.at[j],
+            recv_sem=tp_recv.at[j],
+            device_id={"ep": me, "tp": lax.rem(mt + j, tp)},
+            device_id_type=MESH,
+        )
+
+    for j in range(1, tp):
+        copy = to_tp(j, recv_d.at[mt])
+        copy.start()
+        sends.append(copy)
+    for j in range(1, tp):
+        to_tp(j, recv_d.at[lax.rem(mt + (tp - j), tp)]).wait_recv()
+    mixer = recv_d[0].astype(F32)
+    for j in range(1, tp):
+        mixer = mixer + recv_d[j].astype(F32)
+    residual = (own_cols + mixer).astype(BF16)
+    blocks[me] = residual
+    for k in order:
+        copy = to_ep(3, k, blocks.at[me], blocks.at[me])
+        copy.start()
+        sends.append(copy)
+
+    def gain_of(e):
+        return moe_gain[:, pl.ds(pl.multiple_of(e * col, 128), col)]
+
+    copies["d"].wait()
+    scaled = (residual.astype(F32) * gain_of(me)).astype(BF16)
+    dense_part = jnp.dot(scaled, v_dense[...], preferred_element_type=F32)
+    for e in range(ep):
+        send_g[e] = piece(dense_part, e).astype(BF16)
+    recv_g[me] = send_g[me]
+    for k in order:
+        copy = to_ep(4, k, send_g.at[lax.rem(me + k, ep)], recv_g.at[me])
+        copy.start()
+        sends.append(copy)
+
+    for name in ("g", "u", "w"):
+        copies[name].wait()
+
+    def block_terms(e, block):
+        wide = block.astype(F32)
+        squares = jnp.sum(wide * wide, axis=1, keepdims=True)
+        scaled = (wide * gain_of(e)).astype(BF16)
+        first = pl.multiple_of(e * col, 128)
+        act = jnp.dot(scaled, v_gu[pl.ds(first, col), :], preferred_element_type=F32)
+        logit = lax.dot_general(
+            scaled, small_scr[:, pl.ds(first, col)], last, preferred_element_type=F32
+        )
+        return squares, act, logit
+
+    squares, act, logit = block_terms(me, residual)
+    for k in near:
+        e = source(k)
+        to_ep(3, k, blocks.at[me], blocks.at[e]).wait_recv()
+        more = block_terms(e, blocks[e])
+        squares, act, logit = squares + more[0], act + more[1], logit + more[2]
+    factor = lax.rsqrt(squares * (1.0 / width) + eps)
+    act = act * factor
+    gate = act[:, :ff]
+    hidden = (gate * jax.nn.sigmoid(gate) * act[:, ff:]).astype(BF16)
+    down = jnp.dot(hidden, v_down[...], preferred_element_type=F32)
+    for e in range(ep):
+        for j in range(tp):
+            send_f[e, j] = piece(down, e)[:, j * share : (j + 1) * share].astype(BF16)
+
+    def final(k, j, dst):
+        return pltpu.make_async_remote_copy(
+            src_ref=send_f.at[lax.rem(me + k, ep), lax.rem(mt + j, tp)],
+            dst_ref=dst,
+            send_sem=f_send.at[k, j],
+            recv_sem=f_recv.at[k, j],
+            device_id={"ep": lax.rem(me + k, ep), "tp": lax.rem(mt + j, tp)},
+            device_id_type=MESH,
+        )
+
+    for k in order + [0]:
+        for j in range(tp):
+            if k or j:
+                copy = final(k, j, recv_f.at[me, mt])
+                copy.start()
+                sends.append(copy)
+    recv_f[me, mt] = send_f[me, mt]
+
+    groups = w_group_t.shape[0]
+    spread = jnp.concatenate(
+        [logit * factor, factor, jnp.zeros((every, 128 - 9), F32)]
+        + [blocks[mt * (share // col) + i].astype(F32) for i in range(share // col)],
+        axis=1,
+    )
+    for e in range(ep):
+        rows_scr[e] = piece(spread, e)
+    own = rows_scr[me]
+    group_logit = own[:, :groups]
+    dense_gate = jax.nn.sigmoid(own[:, groups : groups + 1]) * own[:, 8:9]
+    shifted = jnp.exp(group_logit - jnp.max(group_logit, axis=1, keepdims=True))
+    prob = shifted / jnp.sum(shifted, axis=1, keepdims=True)
+    group_lane = lax.broadcasted_iota(jnp.int32, prob.shape, 1)
+    per_group = ep // groups
+    top_count = ids.shape[1]
+    weights = weight[...]
+    total_weight = jnp.sum(weights, axis=1, keepdims=True)
+    lane_e = lax.broadcasted_iota(jnp.int32, (seqs, ep), 1)
+    factor_e = jnp.zeros((seqs, ep), F32)
+    for j in range(top_count):
+        ident = ids[:, j : j + 1]
+        picked = jnp.zeros((seqs, 1), F32)
+        for g in range(groups):
+            inside = (ident >= g * per_group) & (ident < (g + 1) * per_group)
+            picked = picked + jnp.where(inside, prob[:, g : g + 1], 0.0)
+        route = picked * weights[:, j : j + 1] / total_weight
+        factor_e = factor_e + jnp.where(lane_e == ident, route, 0.0)
+
+    for k in near:
+        to_ep(4, k, send_g.at[0], recv_g.at[source(k)]).wait_recv()
+    dense = recv_g[0].astype(F32)
+    for e in range(1, ep):
+        dense = dense + recv_g[e].astype(F32)
+    result = own[:, 128:] + dense_gate * dense
+
+    for k in [0] + near:
+        for j in range(tp):
+            if k or j:
+                final(k, j, recv_f.at[source(k), lax.rem(mt + (tp - j), tp)]).wait_recv()
+    for e in range(ep):
+        expert = recv_f[e, 0].astype(F32)
+        for j in range(1, tp):
+            expert = expert + recv_f[e, j].astype(F32)
+        result = result + factor_e[:, e : e + 1] * expert.astype(BF16).astype(F32)
+    mixed[...] = result.astype(BF16)
+
+    write_c.wait()
+    for copy in sends:
+        copy.wait_send()
+
+
+def fused(ep, tp, *args):
+    (tokens, state_c, state_n, state_m, mix_gain, w_query, w_key, w_value) = args[:8]
+    (w_in, w_forget, forget_bias, w_output, moe_gain, w_group, ids, weight) = args[8:16]
+    (w_gate, w_up, w_down, w_dense, w_dense_gate) = args[16:]
+    seqs, width = tokens.shape
+    qk, vals = w_query.shape[1], w_value.shape[1]
+    col, share, ff = width // ep, width // tp, w_gate.shape[2]
+    every = seqs * ep
+    wide = 2 * qk + vals
+    vmem = pl.BlockSpec(memory_space=pltpu.VMEM)
+    hbm = pl.BlockSpec(memory_space=pl.ANY)
+    operands = [
+        (tokens, vmem),
+        (state_c, hbm),
+        (state_n, vmem),
+        (state_m, vmem),
+        (mix_gain.reshape(1, width), vmem),
+        (w_query, hbm),
+        (w_key, hbm),
+        (w_value, hbm),
+        (w_in.T, vmem),
+        (w_forget.T, vmem),
+        (forget_bias.reshape(1, -1), vmem),
+        (w_output, hbm),
+        (moe_gain.reshape(1, width), vmem),
+        (w_group.T, vmem),
+        (ids, vmem),
+        (weight, vmem),
+        (w_gate, hbm),
+        (w_up, hbm),
+        (w_down, hbm),
+        (w_dense, hbm),
+        (w_dense_gate.reshape(1, width), vmem),
+    ]
+    scratch = [
+        pltpu.VMEM(state_c.shape, F32),
+        pltpu.VMEM((col, wide), BF16),
+        pltpu.VMEM(w_output.shape, BF16),
+        pltpu.VMEM((width, 2 * ff), BF16),
+        pltpu.VMEM((ff, width), BF16),
+        pltpu.VMEM(w_dense.shape, BF16),
+        pltpu.VMEM(state_c.shape, F32),
+        pltpu.VMEM((ep, 2 * seqs, col), BF16),
+        pltpu.VMEM((ep, 2 * seqs, col), BF16),
+        pltpu.VMEM((ep, seqs, wide), BF16),
+        pltpu.VMEM((ep, seqs, wide), BF16),
+        pltpu.VMEM((seqs, vals), BF16),
+        pltpu.VMEM((ep, seqs, vals), BF16),
+        pltpu.VMEM((every, col), BF16),
+        pltpu.VMEM((tp, every, col), BF16),
+        pltpu.VMEM((ep, every, col), BF16),
+        pltpu.VMEM((ep, seqs, share), BF16),
+        pltpu.VMEM((ep, seqs, share), BF16),
+        pltpu.VMEM((ep, tp, seqs, share), BF16),
+        pltpu.VMEM((ep, tp, seqs, share), BF16),
+        pltpu.VMEM((ep, seqs, 128 + share), F32),
+        pltpu.VMEM((8, width), BF16),
+        pltpu.SemaphoreType.DMA((10,)),
+        pltpu.SemaphoreType.DMA((5, ep)),
+        pltpu.SemaphoreType.DMA((5, ep)),
+        pltpu.SemaphoreType.DMA((tp,)),
+        pltpu.SemaphoreType.DMA((tp,)),
+        pltpu.SemaphoreType.DMA((ep, tp)),
+        pltpu.SemaphoreType.DMA((ep, tp)),
+    ]
+    return pl.pallas_call(
+        functools.partial(step_kernel, ep, tp),
+        out_shape=(
+            jax.ShapeDtypeStruct((seqs, share), BF16),
+            jax.ShapeDtypeStruct(state_c.shape, F32),
+            jax.ShapeDtypeStruct(state_n.shape, F32),
+            jax.ShapeDtypeStruct(state_m.shape, F32),
+        ),
+        in_specs=[spec for _, spec in operands],
+        out_specs=(vmem, hbm, vmem, vmem),
+        scratch_shapes=scratch,
+        compiler_params=pltpu.CompilerParams(collective_id=0, has_side_effects=True),
+    )(*[value for value, _ in operands])
+
+
 def solution(mesh):
+    ep, tp = mesh.shape["ep"], mesh.shape["tp"]
+
+    def body(*args):
+        return fused(ep, tp, *args) if fits(ep, tp, args) else per_device(*args)
+
     placed = (
         P("ep", None),
         P("ep", "tp", None, None),
@@ -190,7 +669,7 @@
         P(),
     )
     return jax.shard_map(
-        per_device,
+        body,
         mesh=mesh,
         in_specs=placed,
         out_specs=(P("ep", "tp"), P("ep", "tp", None, None), P("ep", "tp", None), P("ep", "tp")),

time: 202 us -> 41.1 us (0.20)
  blocking collectives: 106 us -> 0 us
  Pallas kernels: 0 us -> 34.5 us
  waiting for transfers between devices: 34.5 us -> 0 us
  starting transfers between devices: 23.1 us -> 0 us
  between operations: 15 us -> 0.66 us
  other arithmetic: 7.76 us -> 0 us
  matrix products: 6.76 us -> 0 us
    unnamed x2 -> x0, blocking collectives: 74.5 us -> none
    pallas_call x0 -> x1, Pallas kernels: none -> 34.5 us  [fused(): pl.pallas_call(functools.partial(step_kernel, ep, tp), out_shape=(jax.Sha...]
    all_gather x1 -> x0, blocking collectives: 26.2 us -> none  [per_device(): lax.all_gather(heads, 'ep', axis=0, tiled=True)]
    all_to_all x5 -> x0, starting transfers between devices: 23.1 us -> none  [the longest x1 7.44 us: per_device(): lax.all_to_all(normed, 'ep', split_axis=1, concat_axis=0, tiled=True)]
    all_to_all x5 -> x0, waiting for transfers between devices: 17.3 us -> none  [the longest x1 6.49 us: per_device(): lax.all_to_all(outgoing, 'ep', split_axis=0, concat_axis=0, tiled=True)]
    reduce_scatter x1 -> x0, waiting for transfers between devices: 17.1 us -> none  [per_device(): lax.psum_scatter(down_part.astype(jnp.bfloat16), 'tp', scatter_dimension=...]
    dot_general x12 -> x0, matrix products: 6.76 us -> none  [the longest x1 1.22 us: per_device(): jnp.dot(token_rows, joined, preferred_element_type=jnp.float32)]
    psum x1 -> x0, blocking collectives: 5.74 us -> none  [per_device(): lax.psum(partial_value.astype(jnp.bfloat16), 'tp').astype(jnp.float32)]
  transfers between devices with their start and end apart: 6 -> 0, of which waited for: 5 -> 0; matrix products, arithmetic and copies ran while one was open for 3% -> 0% of each run, Pallas kernels for 0% -> 0%
where the time goes in v1:
time: 41.1 us; the launch traced here: 40.8 us
  Pallas kernels  34.5 us (84%)
  local copies, waits for them, and re-layouts  5.64 us (14%)
  between operations  0.66 us (2%)
    pallas_call x1, Pallas kernels, fused(): pl.pallas_call(functools.partial(step_kernel, ep, tp), out_shape=(jax.Sha...  34.5 us
    unnamed x12, local copies, waits for them, and re-layouts  5.03 us

profile of v1, /device:TPU:0, one launch (start us, length us, event | category | flops | bytes accessed | tf_op | source)
XLA Modules:
  0.0 40.8 jit_solution(3341459959426812886)
XLA Ops:
  0.6 0.0 copy-start
  0.6 0.7 %copy-done = bf16[2048]{0:T(1024)(128)(2,1)S(1)} copy-done((bf16[2048]{0:T(1024)(128)(2,1)S(1)}, bf16[2048]{0:T(1024)(128)(2,1)}, u32[]{:S(2)}) %copy-start) | copy-done | bytes 4120
  1.3 0.6 %reshape.23.w_dense_gate = bf16[1,2048]{1,0:T(2,128)(2,1)} reshape(bf16[2048]{0:T(1024)(128)(2,1)S(1)} %copy-done) | data formatting | bytes 8192 | tf_op jit(solution)/shard_map/reshape | solution.py:594
  1.9 34.5 %shard_map.228 = (bf16[2,512]{1,0:T(2,128)(2,1)}, f32[2,2,128,256]{3,2,1,0:T(8,128)}, f32[2,2,128]{2,1,0:T(2,128)}, f32[2,2]{1,0:T(2,128)}) custom-call(bf16[2,2048]{1,0:T(2,128)(2,1)} %tokens.1, f32[2,2,128,256]{3,2,1,0:T(8,128)} %state_c.1, f32[2,2,128]{2,1,0:T(2,128)} %state_n.1, f32[2,2]{1,0:T(2,128)} %state_m.1, f32[1,2048]{1,0:T(1,128)} %bitcast.9, ...), custom_call_target="tpu_custom_call" | custom-call | tf_op jit(solution)/shard_map/pallas_call | solution.py:627
  36.4 0.0 copy-start.2
  36.4 0.7 %copy-done.2 = bf16[2,512]{1,0:T(2,128)(2,1)S(1)} copy-done((bf16[2,512]{1,0:T(2,128)(2,1)S(1)}, bf16[2,512]{1,0:T(2,128)(2,1)}, u32[]{:S(2)}) %copy-start.2) | copy-done | bytes 2072
  37.1 0.6 %copy.29 = bf16[2,512]{1,0:T(2,128)(2,1)} copy(bf16[2,512]{1,0:T(2,128)(2,1)S(1)} %copy-done.2) | data formatting | bytes 4096
  37.7 0.0 copy-start.1
  37.7 1.9 %copy.30 = f32[2,2,128,256]{3,2,1,0:T(8,128)} copy(f32[2,2,128,256]{3,2,1,0:T(8,128)} %get-tuple-element.9) | data formatting | bytes 1048576
  39.6 0.0 copy-done.1
  39.6 0.0 copy-start.3
  39.6 0.6 %copy.31 = f32[2,2,128]{2,1,0:T(2,128)} copy(f32[2,2,128]{2,1,0:T(2,128)S(1)} %copy-done.1) | data formatting | bytes 4096
  40.1 0.1 copy-done.3
  40.2 0.6 %copy.32 = f32[2,2]{1,0:T(2,128)} copy(f32[2,2]{1,0:T(2,128)S(1)} %copy-done.3) | data formatting | bytes 32
Async XLA Ops:
  0.6 0.7 %copy-start = (bf16[2048]{0:T(1024)(128)(2,1)S(1)}, bf16[2048]{0:T(1024)(128)(2,1)}, u32[]{:S(2)}) copy-start(bf16[2048]{0:T(1024)(128)(2,1)} %param.41) | copy-start | bytes 12292
  36.4 0.7 %copy-start.2 = (bf16[2,512]{1,0:T(2,128)(2,1)S(1)}, bf16[2,512]{1,0:T(2,128)(2,1)}, u32[]{:S(2)}) copy-start(bf16[2,512]{1,0:T(2,128)(2,1)} %get-tuple-element.8) | copy-start | bytes 6148
  37.7 1.9 %copy-start.1 = (f32[2,2,128]{2,1,0:T(2,128)S(1)}, f32[2,2,128]{2,1,0:T(2,128)}, u32[]{:S(2)}) copy-start(f32[2,2,128]{2,1,0:T(2,128)} %get-tuple-element.10) | copy-start | bytes 6148
  39.6 0.7 %copy-start.3 = (f32[2,2]{1,0:T(2,128)S(1)}, f32[2,2]{1,0:T(2,128)}, u32[]{:S(2)}) copy-start(f32[2,2]{1,0:T(2,128)} %get-tuple-element.11) | copy-start | bytes 52

commit v2 on v1

--- a/solution.py
+++ b/solution.py
@@ -225,7 +225,6 @@
     v_gu,
     v_down,
     v_dense,
-    new_c,
     send_a,
     recv_a,
     send_b,
@@ -385,7 +384,7 @@
             q_col = upright[:, at : at + 1]
             k_col = upright[:, count + at : count + at + 1]
             fresh = decay * v_c[s, h] + k_col * v_rows[at]
-            new_c[s, h] = fresh
+            out_c[s, h] = fresh
             numer = jnp.sum(q_col * fresh, axis=0, keepdims=True)
             fresh_n = decay * state_n[s, h : h + 1] + k_rows[at]
             out_n[s, h : h + 1] = fresh_n
@@ -399,13 +398,15 @@
         copy = to_ep(2, k, send_c, recv_c.at[me])
         copy.start()
         sends.append(copy)
-    write_c = pltpu.make_async_copy(new_c, out_c, local_sem.at[len(plan)])
-    write_c.start()
-
+
+    gate_rows = w_dense_gate[...].astype(F32)
+    gate_row = jnp.concatenate(
+        [gate_rows[i : i + 1] for i in range(width // 128)], axis=1
+    )
     small = jnp.concatenate(
         [
             w_group_t[...].astype(F32),
-            w_dense_gate[...].astype(F32),
+            gate_row,
             jnp.zeros((8 - w_group_t.shape[0] - 1, width), F32),
         ],
         axis=0,
@@ -554,7 +555,6 @@
         result = result + factor_e[:, e : e + 1] * expert.astype(BF16).astype(F32)
     mixed[...] = result.astype(BF16)
 
-    write_c.wait()
     for copy in sends:
         copy.wait_send()
 
@@ -569,7 +569,7 @@
     every = seqs * ep
     wide = 2 * qk + vals
     vmem = pl.BlockSpec(memory_space=pltpu.VMEM)
-    hbm = pl.BlockSpec(memory_space=pl.ANY)
+    hbm = pl.BlockSpec(memory_space=pltpu.HBM)
     operands = [
         (tokens, vmem),
         (state_c, hbm),
@@ -591,7 +591,7 @@
         (w_up, hbm),
         (w_down, hbm),
         (w_dense, hbm),
-        (w_dense_gate.reshape(1, width), vmem),
+        (w_dense_gate.reshape(-1, 128), vmem),
     ]
     scratch = [
         pltpu.VMEM(state_c.shape, F32),
@@ -600,7 +600,6 @@
         pltpu.VMEM((width, 2 * ff), BF16),
         pltpu.VMEM((ff, width), BF16),
         pltpu.VMEM(w_dense.shape, BF16),
-        pltpu.VMEM(state_c.shape, F32),
         pltpu.VMEM((ep, 2 * seqs, col), BF16),
         pltpu.VMEM((ep, 2 * seqs, col), BF16),
         pltpu.VMEM((ep, seqs, wide), BF16),
@@ -624,19 +623,40 @@
         pltpu.SemaphoreType.DMA((ep, tp)),
         pltpu.SemaphoreType.DMA((ep, tp)),
     ]
+    outs = (
+        jax.ShapeDtypeStruct((seqs, share), BF16),
+        jax.ShapeDtypeStruct(state_c.shape, F32),
+        jax.ShapeDtypeStruct(state_n.shape, F32),
+        jax.ShapeDtypeStruct(state_m.shape, F32),
+    )
+    spare = 4 * state_c.size + (20 << 10)
+    kept = pl.pallas_call(
+        functools.partial(step_kernel, ep, tp),
+        out_shape=tuple(pltpu.VMEM(out.shape, out.dtype) for out in outs),
+        in_specs=[spec for _, spec in operands],
+        out_specs=(vmem,) * 4,
+        scratch_shapes=scratch,
+        compiler_params=pltpu.CompilerParams(
+            collective_id=0, has_side_effects=True, vmem_limit_bytes=67043328 - spare
+        ),
+    )(*[value for value, _ in operands])
     return pl.pallas_call(
-        functools.partial(step_kernel, ep, tp),
-        out_shape=(
-            jax.ShapeDtypeStruct((seqs, share), BF16),
-            jax.ShapeDtypeStruct(state_c.shape, F32),
-            jax.ShapeDtypeStruct(state_n.shape, F32),
-            jax.ShapeDtypeStruct(state_m.shape, F32),
-        ),
-        in_specs=[spec for _, spec in operands],
-        out_specs=(vmem, hbm, vmem, vmem),
-        scratch_shapes=scratch,
-        compiler_params=pltpu.CompilerParams(collective_id=0, has_side_effects=True),
-    )(*[value for value, _ in operands])
+        write_out,
+        out_shape=outs,
+        in_specs=[vmem] * 4,
+        out_specs=(pl.BlockSpec(memory_space=pltpu.HBM),) * 4,
+        scratch_shapes=[pltpu.SemaphoreType.DMA((4,))],
+        compiler_params=pltpu.CompilerParams(vmem_limit_bytes=4 << 20),
+    )(*kept)
+
+
+def write_out(*refs):
+    sems = refs[-1]
+    copies = [pltpu.make_async_copy(refs[i], refs[4 + i], sems.at[i]) for i in range(4)]
+    for copy in copies:
+        copy.start()
+    for copy in copies:
+        copy.wait()
 
 
 def solution(mesh):

time: 41.1 us -> 35.6 us (0.87)
  local copies, waits for them, and re-layouts: 5.64 us -> 0 us
    unnamed x12 -> x0, local copies, waits for them, and re-layouts: 5.03 us -> none
    reshape x1 -> x0, local copies, waits for them, and re-layouts: 0.6 us -> none  [fused(): w_dense_gate.reshape(1, width)]
    pallas_call x1 -> x2, Pallas kernels: 34.5 us -> 34.7 us  [the longest x1 33.9 us: fused(): pl.pallas_call(functools.partial(step_kernel, ep, tp), out_shape=tuple((p...]
where the time goes in v2:
time: 35.6 us; the launch traced here: 35.4 us
  Pallas kernels  34.7 us (97%)
  between operations  0.65 us (2%)
    pallas_call x1, Pallas kernels, fused(): pl.pallas_call(functools.partial(step_kernel, ep, tp), out_shape=tuple((p...  33.9 us
    pallas_call x1, Pallas kernels, fused(): pl.pallas_call(write_out, out_shape=outs, in_specs=[vmem] * 4, out_specs=...  0.84 us

profile of v2, /device:TPU:0, one launch (start us, length us, event | category | flops | bytes accessed | tf_op | source)
XLA Modules:
  0.0 35.4 jit_solution(2616150950910746259)
XLA Ops:
  0.6 33.9 %shard_map.228 = (bf16[2,512]{1,0:T(2,128)(2,1)S(1)}, f32[2,2,128,256]{3,2,1,0:T(8,128)S(1)}, f32[2,2,128]{2,1,0:T(2,128)S(1)}, f32[2,2]{1,0:T(2,128)S(1)}) custom-call(bf16[2,2048]{1,0:T(2,128)(2,1)} %tokens.1, f32[2,2,128,256]{3,2,1,0:T(8,128)} %state_c.1, f32[2,2,128]{2,1,0:T(2,128)} %state_n.1, f32[2,2]{1,0:T(2,128)} %state_m.1, f32[1,2048]{1,0:T(1,128)} %bitcast.10, ...), custom_call_target="tpu_custom_call" | custom-call | tf_op jit(solution)/shard_map/pallas_call | solution.py:633
  34.6 0.8 %shard_map.229 = (bf16[2,512]{1,0:T(2,128)(2,1)}, f32[2,2,128,256]{3,2,1,0:T(8,128)}, f32[2,2,128]{2,1,0:T(2,128)}, f32[2,2]{1,0:T(2,128)}) custom-call(bf16[2,512]{1,0:T(2,128)(2,1)S(1)} %get-tuple-element.8.refs_0_, f32[2,2,128,256]{3,2,1,0:T(8,128)S(1)} %get-tuple-element.9.refs_1_, f32[2,2,128]{2,1,0:T(2,128)S(1)} %get-tuple-element.10.refs_2_, ...), custom_call_target="tpu_custom_call" | custom-call | tf_op jit(solution)/shard_map/pallas_call | solution.py:643

commit v3 on v2

--- a/solution.py
+++ b/solution.py
@@ -169,6 +169,7 @@
     return (mixed, new_c, new_n, new_m)
 
 
+SMALL = (0, 2, 3, 4, 8, 9, 10, 12, 13, 14, 15, 20)
 F32 = jnp.float32
 BF16 = jnp.bfloat16
 MESH = pl.DeviceIdType.MESH
@@ -194,31 +195,43 @@
 def step_kernel(
     ep,
     tp,
+    h_tokens,
+    state_c,
+    h_state_n,
+    h_state_m,
+    h_mix_gain,
+    w_query,
+    w_key,
+    w_value,
+    h_w_in_t,
+    h_w_forget_t,
+    h_forget_bias,
+    w_output,
+    h_moe_gain,
+    h_w_group_t,
+    h_ids,
+    h_weight,
+    w_gate,
+    w_up,
+    w_down,
+    w_dense,
+    h_w_dense_gate,
+    mixed,
+    out_c,
+    out_n,
+    out_m,
     tokens,
-    state_c,
     state_n,
     state_m,
     mix_gain,
-    w_query,
-    w_key,
-    w_value,
     w_in_t,
     w_forget_t,
     forget_bias,
-    w_output,
     moe_gain,
     w_group_t,
     ids,
     weight,
-    w_gate,
-    w_up,
-    w_down,
-    w_dense,
     w_dense_gate,
-    mixed,
-    out_c,
-    out_n,
-    out_m,
     v_c,
     v_qkv,
     v_out,
@@ -259,32 +272,44 @@
     ff = w_gate.shape[2]
     every = ep * seqs
 
-    copies = {}
-    plan = [
-        ("q", w_query, v_qkv.at[:, 0:qk]),
-        ("k", w_key, v_qkv.at[:, qk : 2 * qk]),
-        ("v", w_value, v_qkv.at[:, 2 * qk :]),
-        ("c", state_c, v_c),
-        ("o", w_output, v_out),
-        ("d", w_dense, v_dense),
-        ("g", w_gate.at[0], v_gu.at[:, 0:ff]),
-        ("u", w_up.at[0], v_gu.at[:, ff:]),
-        ("w", w_down.at[0], v_down),
-    ]
-    for number, (name, src, dst) in enumerate(plan):
-        copies[name] = pltpu.make_async_copy(src, dst, local_sem.at[number])
-        copies[name].start()
-
     barrier = pltpu.get_barrier_semaphore()
     for k in range(ep):
         for j in range(tp):
-            if k or j:
+            if (k == 0) != (j == 0):
                 pl.semaphore_signal(
                     barrier,
                     inc=1,
                     device_id={"ep": lax.rem(me + k, ep), "tp": lax.rem(mt + j, tp)},
                     device_id_type=MESH,
                 )
+
+    copies = {}
+    plan = [
+        ("tokens", h_tokens, tokens),
+        ("mix_gain", h_mix_gain, mix_gain),
+        ("q", w_query, v_qkv.at[:, 0:qk]),
+        ("k", w_key, v_qkv.at[:, qk : 2 * qk]),
+        ("v", w_value, v_qkv.at[:, 2 * qk :]),
+        ("w_in_t", h_w_in_t, w_in_t),
+        ("w_forget_t", h_w_forget_t, w_forget_t),
+        ("forget_bias", h_forget_bias, forget_bias),
+        ("state_m", h_state_m, state_m),
+        ("c", state_c, v_c),
+        ("state_n", h_state_n, state_n),
+        ("o", w_output, v_out),
+        ("d", w_dense, v_dense),
+        ("g", w_gate.at[0], v_gu.at[:, 0:ff]),
+        ("u", w_up.at[0], v_gu.at[:, ff:]),
+        ("w", w_down.at[0], v_down),
+        ("moe_gain", h_moe_gain, moe_gain),
+        ("w_group_t", h_w_group_t, w_group_t),
+        ("w_dense_gate", h_w_dense_gate, w_dense_gate),
+        ("ids", h_ids, ids),
+        ("weight", h_weight, weight),
+    ]
+    for number, (name, src, dst) in enumerate(plan):
+        copies[name] = pltpu.make_async_copy(src, dst, local_sem.at[number])
+        copies[name].start()
 
     def to_ep(phase, k, src, dst):
         return pltpu.make_async_remote_copy(
@@ -300,6 +325,8 @@
         return lax.rem(me + (ep - k), ep)
 
     sends = []
+    copies["tokens"].wait()
+    copies["mix_gain"].wait()
     tok = tokens[...].astype(F32)
     inverse = lax.rsqrt(jnp.mean(tok * tok, axis=-1, keepdims=True) + eps)
     normed_f = tok * inverse * mix_gain[...]
@@ -309,7 +336,7 @@
         send_a[e] = both[:, e * col : (e + 1) * col]
     recv_a[me] = send_a[me]
 
-    pl.semaphore_wait(barrier, ep * tp - 1)
+    pl.semaphore_wait(barrier, ep + tp - 2)
 
     order = sorted(range(1, ep), key=lambda k: -min(k, ep - k))
     near = order[::-1]
@@ -318,6 +345,8 @@
         copy.start()
         sends.append(copy)
 
+    for name in ("w_in_t", "w_forget_t", "forget_bias", "state_m"):
+        copies[name].wait()
     last = (((1,), (1,)), ((), ()))
     gate_all = lax.dot_general(normed, w_in_t[...], last, preferred_element_type=F32)
     pre = lax.dot_general(normed, w_forget_t[...], last, preferred_element_type=F32)
@@ -357,6 +386,7 @@
         sends.append(copy)
 
     copies["c"].wait()
+    copies["state_n"].wait()
     for k in near:
         to_ep(1, k, send_b.at[0], recv_b.at[source(k)]).wait_recv()
     summed = recv_b[0].astype(F32)
@@ -399,6 +429,8 @@
         copy.start()
         sends.append(copy)
 
+    for name in ("moe_gain", "w_group_t", "w_dense_gate", "ids", "weight"):
+        copies[name].wait()
     gate_rows = w_dense_gate[...].astype(F32)
     gate_row = jnp.concatenate(
         [gate_rows[i : i + 1] for i in range(width // 128)], axis=1
@@ -571,29 +603,29 @@
     vmem = pl.BlockSpec(memory_space=pltpu.VMEM)
     hbm = pl.BlockSpec(memory_space=pltpu.HBM)
     operands = [
-        (tokens, vmem),
+        (tokens, hbm),
         (state_c, hbm),
-        (state_n, vmem),
-        (state_m, vmem),
-        (mix_gain.reshape(1, width), vmem),
+        (state_n, hbm),
+        (state_m, hbm),
+        (mix_gain.reshape(1, width), hbm),
         (w_query, hbm),
         (w_key, hbm),
         (w_value, hbm),
-        (w_in.T, vmem),
-        (w_forget.T, vmem),
-        (forget_bias.reshape(1, -1), vmem),
+        (w_in.T, hbm),
+        (w_forget.T, hbm),
+        (forget_bias.reshape(1, -1), hbm),
         (w_output, hbm),
-        (moe_gain.reshape(1, width), vmem),
-        (w_group.T, vmem),
-        (ids, vmem),
-        (weight, vmem),
+        (moe_gain.reshape(1, width), hbm),
+        (w_group.T, hbm),
+        (ids, hbm),
+        (weight, hbm),
         (w_gate, hbm),
         (w_up, hbm),
         (w_down, hbm),
         (w_dense, hbm),
-        (w_dense_gate.reshape(-1, 128), vmem),
+        (w_dense_gate.reshape(-1, 128), hbm),
     ]
-    scratch = [
+    scratch = [pltpu.VMEM(operands[i][0].shape, operands[i][0].dtype) for i in SMALL] + [
         pltpu.VMEM(state_c.shape, F32),
         pltpu.VMEM((col, wide), BF16),
         pltpu.VMEM(w_output.shape, BF16),
@@ -615,7 +647,7 @@
         pltpu.VMEM((ep, tp, seqs, share), BF16),
         pltpu.VMEM((ep, seqs, 128 + share), F32),
         pltpu.VMEM((8, width), BF16),
-        pltpu.SemaphoreType.DMA((10,)),
+        pltpu.SemaphoreType.DMA((len(operands),)),
         pltpu.SemaphoreType.DMA((5, ep)),
         pltpu.SemaphoreType.DMA((5, ep)),
         pltpu.SemaphoreType.DMA((tp,)),

time: 35.6 us -> 34.7 us (0.975)
  Pallas kernels: 34.7 us -> 33.8 us
    pallas_call x1, Pallas kernels: 33.9 us -> 33 us  [fused(): pl.pallas_call(functools.partial(step_kernel, ep, tp), out_shape=tuple((p...]
where the time goes in v3:
time: 34.7 us; the launch traced here: 34.5 us
  Pallas kernels  33.8 us (97%)
  between operations  0.65 us (2%)
    pallas_call x1, Pallas kernels, fused(): pl.pallas_call(functools.partial(step_kernel, ep, tp), out_shape=tuple((p...  33 us
    pallas_call x1, Pallas kernels, fused(): pl.pallas_call(write_out, out_shape=outs, in_specs=[vmem] * 4, out_specs=...  0.84 us

profile of v3, /device:TPU:0, one launch (start us, length us, event | category | flops | bytes accessed | tf_op | source)
XLA Modules:
  0.0 34.5 jit_solution(15560992171385029475)
XLA Ops:
  0.6 33.0 %shard_map.228 = (bf16[2,512]{1,0:T(2,128)(2,1)S(1)}, f32[2,2,128,256]{3,2,1,0:T(8,128)S(1)}, f32[2,2,128]{2,1,0:T(2,128)S(1)}, f32[2,2]{1,0:T(2,128)S(1)}) custom-call(bf16[2,2048]{1,0:T(2,128)(2,1)} %h_tokens.1, f32[2,2,128,256]{3,2,1,0:T(8,128)} %state_c.1, f32[2,2,128]{2,1,0:T(2,128)} %h_state_n.1, f32[2,2]{1,0:T(2,128)} %h_state_m.1, ...), custom_call_target="tpu_custom_call" | custom-call | tf_op jit(solution)/shard_map/pallas_call | solution.py:665
  33.6 0.8 %shard_map.229 = (bf16[2,512]{1,0:T(2,128)(2,1)}, f32[2,2,128,256]{3,2,1,0:T(8,128)}, f32[2,2,128]{2,1,0:T(2,128)}, f32[2,2]{1,0:T(2,128)}) custom-call(bf16[2,512]{1,0:T(2,128)(2,1)S(1)} %get-tuple-element.8.refs_0_, f32[2,2,128,256]{3,2,1,0:T(8,128)S(1)} %get-tuple-element.9.refs_1_, f32[2,2,128]{2,1,0:T(2,128)S(1)} %get-tuple-element.10.refs_2_, ...), custom_call_target="tpu_custom_call" | custom-call | tf_op jit(solution)/shard_map/pallas_call | solution.py:675
